TPU v7x, 512 devices: a 4x2x32 block of a 4x8x32 slice. The times are simulated.
512 devices in a mesh: grp: 2 (over y), sp: 64 (over z, core), tp: 4 (over x).
Axes of the slice: x: 4, y: 2, z: 32, core: 2. Of those that a mesh axis runs over, the one named last changes fastest.
The devices are a block of a 4x8x32 slice.
Arguments:
- tokens: bfloat16 [49152, 2048], P(('grp', 'sp')), parts along dimension 0, may hold values from -6 to 6
- norm_gain: float32 [2, 2048], replicated, may hold values from 0.1 to 1.9
- entry_weight: bfloat16 [2, 2048, 2048], P(None, 'sp', 'tp'), may hold values from -0.125 to 0.125
- mix_weight: bfloat16 [2, 4, 512, 512], P(None, 'tp'), may hold values from -0.25 to 0.25
- pool_gain: float32 [2, 2048], P(None, 'tp'), may hold values from 0.1 to 1.9
- back_weight: bfloat16 [2, 2048, 2048], P(None, 'tp', 'sp'), may hold values from -0.25 to 0.25
Outputs:
- result_tokens: bfloat16 [49152, 2048], P(('grp', 'sp')), parts along dimension 0
There are 2 independent parts, one for each index of `grp`. A program takes and returns all parts, laid end to end along the dimension named above; an argument that names none is the same for every part. Nothing has to cross between parts.
All inputs are finite; a program needn't handle non-finite values.
Results may differ from a plain program's by a relative error of at most 0.018.
Values may be sent and summed in bfloat16 or wider, within the bound.
A program may use at most 64 MiB of HBM per device.

v0:
```python
import jax
import jax.numpy as jnp
from jax import lax
from jax.sharding import PartitionSpec as P

GROUPS = 4
LAYERS = 2


EPSILON = 1e-05


def extended_2(value, sides, width):
    for axis, dim in sides:
        size, length = (lax.axis_size(axis), value.shape[dim])
        up = [(i, (i + 1) % size) for i in range(size - 1)]
        down = [(j, i) for i, j in up]
        last = lax.slice_in_dim(value, length - width, length, axis=dim)
        first = lax.slice_in_dim(value, 0, width, axis=dim)
        before = lax.ppermute(last, axis, up)
        after = lax.ppermute(first, axis, down)
        value = jnp.concatenate([before, value, after], axis=dim)
    return value


def gather_turned(arrays, axis, dims):
    turned = [jnp.moveaxis(a, dim, 0) for a, dim in zip(arrays, dims)]
    both = jnp.concatenate([t.reshape(len(t), -1) for t in turned], axis=1)
    out, at, done = (lax.all_gather(both, axis, axis=0, tiled=True), 0, [])
    for t, dim in zip(turned, dims):
        section = out[:, at : at + t[0].size].reshape(-1, *t.shape[1:])
        done.append(jnp.moveaxis(section, 0, dim))
        at += t[0].size
    return tuple(done)


def from_everyone(value, axis):
    length = lax.axis_size(axis)
    return lax.all_to_all(
        jnp.broadcast_to(value[None], (length, *value.shape)), axis, 0, 0, tiled=True
    )


def over_copies(value, axis):
    everything = from_everyone(value, axis)
    return jnp.sum(everything.astype(jnp.float32), axis=0)


def window_mean(padded, positions, halves, total_length, reach):
    row_count = positions.shape[0]
    summed = jnp.zeros((row_count,) + padded.shape[1:], jnp.float32)
    for offset in range(-reach, reach):
        inside = ((offset >= -halves) & (offset < halves)).astype(jnp.float32)
        summed = (
            summed + padded[reach + offset : reach + offset + row_count] * inside[None, :, None]
        )
    lower = jnp.maximum(positions[:, None] - halves[None, :], 0)
    upper = jnp.minimum(positions[:, None] + halves[None, :], total_length)
    counted = (upper - lower).astype(jnp.float32)
    return summed / counted[:, :, None]


def normalize(state, gain):
    values = state.astype(jnp.float32)
    scaled = values * lax.rsqrt(jnp.mean(values * values, axis=-1, keepdims=True) + EPSILON)
    return (scaled * gain).astype(jnp.bfloat16)


def pool_groups(pooled_in, mix_layer, gain_layer, reach):
    row_count = pooled_in.shape[0]
    group_here = mix_layer.shape[0]
    width = mix_layer.shape[1]
    extended = extended_2(pooled_in, (("sp", 0),), reach)
    first_group = lax.axis_index("tp") * group_here
    halves = jnp.left_shift(jnp.int32(1), first_group + jnp.arange(group_here, dtype=jnp.int32))
    positions = lax.axis_index("sp") * row_count + jnp.arange(row_count, dtype=jnp.int32)
    total_length = lax.axis_size("sp") * row_count
    padded = extended.reshape(row_count + 2 * reach, group_here, width).astype(jnp.float32)
    means = window_mean(padded, positions, halves, total_length, reach)
    differ = (means - padded[reach : reach + row_count]).astype(jnp.bfloat16)
    mixed = jnp.einsum("tgc,gcd->tgd", differ, mix_layer, preferred_element_type=jnp.float32)
    return (mixed.reshape(row_count, group_here * width) * gain_layer).astype(jnp.bfloat16)


def per_device(tokens, norm_gain, entry_weight, mix_weight, pool_gain, back_weight):
    reach = 2 ** (GROUPS - 1)
    state = tokens
    entry_all, back_all = gather_turned((entry_weight, back_weight), "sp", (1, 2))
    for layer in range(LAYERS):
        normed = normalize(state, norm_gain[layer])
        pooled_in = jnp.dot(normed, entry_all[layer], preferred_element_type=jnp.float32).astype(
            jnp.bfloat16
        )
        back_local = back_all[layer]
        mixed = pool_groups(pooled_in, mix_weight[layer], pool_gain[layer], reach)
        update = jnp.dot(mixed, back_local, preferred_element_type=jnp.float32)
        summed = over_copies(update.astype(jnp.bfloat16), "tp").astype(jnp.float32)
        state = (state.astype(jnp.float32) + summed).astype(jnp.bfloat16)
    return state


def solution(mesh):
    return jax.shard_map(
        per_device,
        mesh=mesh,
        in_specs=(
            P(("grp", "sp"), None),
            P(),
            P(None, "sp", "tp"),
            P(None, "tp", None, None),
            P(None, "tp"),
            P(None, "tp", "sp"),
        ),
        out_specs=P(("grp", "sp"), None),
        check_vma=False,
    )
```

profile of v0, /device:TPU:40, one launch (start us, length us, event | category | flops | bytes accessed | tf_op | source)
XLA Modules:
  0.0 389.7 jit_solution(11383457933430418808)
XLA Ops:
  6.6 0.8 copy.17
  7.4 0.8 copy.18
  9.0 1.8 fusion
  12.4 162.8 %all-gather.2.cloned.1.call-done = bf16[2048,2048]{1,0:T(8,128)(2,1)} async-done(((bf16[32,2048]{1,0:T(8,128)(2,1)}), bf16[2048,2048]{1,0:T(8,128)(2,1)}) %all-gather.2.cloned.1.call-update) | async-done | bytes 8388624 | tf_op jit(solution)/shard_map/all_gather | solution.py:29
  175.2 5.2 %fusion.83 = (bf16[2048,1024]{1,0:T(8,128)(2,1)S(1)}, bf16[2048,1024]{1,0:T(8,128)(2,1)}) fusion(bf16[2048,2048]{1,0:T(8,128)(2,1)} %all-gather.2.cloned.1.call-done), kind=kLoop, calls=%fused_computation.119 | loop fusion | bytes 16777216 | tf_op jit(solution)/shard_map/slice | solution.py:31
  180.8 1.3 copy-done
  182.1 1.0 fusion.20
  183.2 2.2 collective-permute-start
  185.3 1.3 collective-permute-start.1
  186.8 6.6 %copy.15 = bf16[2048,1024]{0,1:T(8,128)(2,1)} copy(bf16[2048,1024]{1,0:T(8,128)(2,1)} %get-tuple-element.8) | data formatting | bytes 8388608 | tf_op jit(solution)/shard_map/reshape | solution.py:31
  193.3 1.0 maximum_convert_fusion
  194.3 11.0 %convolution_convert_fusion.1 = bf16[384,2048]{1,0:T(8,128)(2,1)S(1)} fusion(bf16[2,512,2048]{2,1,0:T(8,128)(2,1)} %bitcast.97, bf16[2,1,512,512]{3,2,1,0:T(8,128)(2,1)} %param.9, f32[512]{0:T(512)S(1)} %bitcast.112, f32[400,1,512]{2,0,1:T(8,128)} %maximum_convert_fusion, f32[384]{0:T(512)S(1)} %subtract_convert_fusion, f32[]{:T(128)S(6)} %mul.373, ...), kind=kOutput, calls=%fused_computation.18 | convolution fusion | flops 1014497280 | bytes 16780864 | tf_op jit(solution)/shard_map/dot_general | solution.py:96
  206.1 76.4 %all_to_all.10 = bf16[4,384,2048]{2,1,0:T(8,128)(2,1)S(1)} all-to-all(bf16[4,384,2048]{2,1,0:T(8,128)(2,1)S(1)} %broadcast_in_dim.4), channel_id=1, replica_groups=mesh['grp'=2,'sp'=64,'tp'=4] {'tp'}, dimensions={0} | all-to-all | bytes 12582912 | tf_op jit(solution)/shard_map/all_to_all | solution.py:39
  282.5 1.3 convert_reduce_fusion.1
  284.3 1.6 copy-done.2
  286.0 1.0 fusion.23
  287.0 1.9 collective-permute-start.2
  289.0 1.5 collective-permute-start.3
  290.5 2.7 collective-permute-done.3
  293.2 1.0 maximum_convert_fusion.1
  294.2 11.0 %convolution_convert_fusion = bf16[384,2048]{1,0:T(8,128)(2,1)S(1)} fusion(bf16[2,512,2048]{2,1,0:T(8,128)(2,1)} %bitcast.98, bf16[2,1,512,512]{3,2,1,0:T(8,128)(2,1)} %param.9, f32[512]{0:T(512)S(1)} %bitcast.111, f32[400,1,512]{2,0,1:T(8,128)} %maximum_convert_fusion.1, f32[384]{0:T(512)S(1)} %subtract_convert_fusion, f32[]{:T(128)S(6)} %mul.373, ...), kind=kOutput, calls=%fused_computation.17 | convolution fusion | flops 1014497280 | bytes 16780864 | tf_op jit(solution)/shard_map/dot_general | solution.py:96
  306.0 73.9 %all_to_all.11 = bf16[4,384,2048]{2,1,0:T(8,128)(2,1)S(1)} all-to-all(bf16[4,384,2048]{2,1,0:T(8,128)(2,1)S(1)} %broadcast_in_dim.5), channel_id=1, replica_groups=mesh['grp'=2,'sp'=64,'tp'=4] {'tp'}, dimensions={0} | all-to-all | bytes 12582912 | tf_op jit(solution)/shard_map/all_to_all | solution.py:39
  379.9 1.3 convert_reduce_fusion
  381.2 1.6 fusion.7
  (21 shorter events, 4.8 us)
Async XLA Ops:
  6.5 168.6 %all-gather.2.cloned.1.call-start = ((), (), s32[]{:S(2)}) async-start(), calls=%async_computation.2 | async-start | bytes 8519680 | tf_op jit(solution)/shard_map/all_gather | solution.py:29
  180.4 1.7 copy-start
  180.8 2.4 copy-start.1
  183.2 10.2 %collective-permute-start = (bf16[8,512]{1,0:T(8,128)(2,1)S(1)}, bf16[8,512]{1,0:T(8,128)(2,1)S(1)}, u32[]{:S(2)}, u32[]{:S(2)}) collective-permute-start(bf16[8,512]{1,0:T(8,128)(2,1)S(1)} %get-tuple-element.11), channel_id=1, source_target_pairs={{0,4},{4,8},{8,12},{12,16},{16,20},{20,24},{24,28},{28,32},{32,36}... | collective-permute-start | bytes 24584 | tf_op jit(solution)/shard_map/ppermute | solution.py:20
  185.3 8.0 %collective-permute-start.1 = (bf16[8,512]{1,0:T(8,128)(2,1)S(1)}, bf16[8,512]{1,0:T(8,128)(2,1)S(1)}, u32[]{:S(2)}, u32[]{:S(2)}) collective-permute-start(bf16[8,512]{1,0:T(8,128)(2,1)S(1)} %get-tuple-element.12), channel_id=1, source_target_pairs={{4,0},{8,4},{12,8},{16,12},{20,16},{24,20},{28,24},{32,28},{36,32}... | collective-permute-start | bytes 24584 | tf_op jit(solution)/shard_map/ppermute | solution.py:21
  283.8 2.2 copy-start.2
  287.0 3.4 collective-permute-start.2
  289.0 4.2 %collective-permute-start.3 = (bf16[8,512]{1,0:T(8,128)(2,1)S(1)}, bf16[8,512]{1,0:T(8,128)(2,1)S(1)}, u32[]{:S(2)}, u32[]{:S(2)}) collective-permute-start(bf16[8,512]{1,0:T(8,128)(2,1)S(1)} %get-tuple-element.10), channel_id=1, source_target_pairs={{4,0},{8,4},{12,8},{16,12},{20,16},{24,20},{28,24},{32,28},{36,32}... | collective-permute-start | bytes 24584 | tf_op jit(solution)/shard_map/ppermute | solution.py:21
Sparse Core Ops, SparseCore 0:
  9.5 165.6 all-gather.1
where the time goes:
time: 393 us; the launch traced here: 390 us
  waiting for transfers between devices  166 us (42%)
  blocking collectives  150 us (38%)
  matrix products  24 us (6%)
  local copies, waits for them, and re-layouts  19.9 us (5%)
  between operations  13.7 us (3%)
  other arithmetic  9.18 us (2%)
  starting transfers between devices  6.9 us (2%)
    all_gather x1, waiting for transfers between devices, gather_turned(): out, at, done = (lax.all_gather(both, axis, axis=0, tiled=True), 0, [])  163 us
    all_to_all x2, blocking collectives, from_everyone(): lax.all_to_all(jnp.broadcast_to(value[None], (length, *value.shape)), axi...  150 us
    dot_general x2, matrix products, per_device(): update = jnp.dot(mixed, back_local, preferred_element_type=jnp.float32)  21.9 us
  transfers between devices with their start and end apart: 5, of which 2 were waited for; matrix products, arithmetic and copies ran while one was open for 3% of the time, Pallas kernels for 0%

commit v1 on v0

v1 whole, which is shorter than its diff:
```python
import functools

import jax
import jax.numpy as jnp
from jax import lax
from jax.experimental import pallas as pl
from jax.experimental.pallas import tpu as pltpu
from jax.sharding import PartitionSpec as P

GROUPS = 4
LAYERS = 2
EPSILON = 1e-05
MESH = pl.DeviceIdType.MESH
REACH = 2 ** (GROUPS - 1)
HALO = LAYERS * REACH
CHUNKS = 2
CORES = 2
PIECES = 2 * LAYERS
TILE = 16


def half_rows(rows):
    return (rows // 2 + TILE - 1) // TILE * TILE


def kernel(
    nsp, ntp, tok, weights, norm_gain, mix, pool_gain, out,
    ext, w_all, normed, pooled, mixed,
    term0, term1, acc0, acc1, via_left0, via_left1, via_right0, via_right1,
    from_left0, from_left1, from_right0, from_right1, state0, state1,
    z_send, z_recv, p_send, p_recv, h_send, h_recv, x_send, x_recv, l_sem, o_sem,
):
    rows, model = tok.shape
    width = model // ntp // CHUNKS
    block = weights.shape[1]
    nz = nsp // CORES
    sp = lax.axis_index("sp")
    me = lax.axis_index("tp")
    z, core = sp // CORES, lax.rem(sp, CORES)
    total_length = nsp * rows
    term, acc = (term0, term1), (acc0, acc1)
    via_left, via_right = (via_left0, via_left1), (via_right0, via_right1)
    from_left, from_right = (from_left0, from_left1), (from_right0, from_right1)
    state = (state0, state1)

    def around(value, size):
        return lax.rem(value + size, size)

    z_next = (around(z + 1, nz) * CORES + core, around(z - 1, nz) * CORES + core)
    partner = z * CORES + (1 - core)
    seq_left, seq_right = around(sp - 1, nsp), around(sp + 1, nsp)
    tp_right, tp_left, tp_far = around(me + 1, ntp), around(me - 1, ntp), around(me + 2, ntp)

    barrier = pltpu.get_barrier_semaphore()
    far = jnp.where(core == 0, seq_left, seq_right)
    for target in (z_next[0], z_next[1], partner, far):
        pl.semaphore_signal(barrier, inc=1, device_id={"sp": target}, device_id_type=MESH)
    for target in (tp_right, tp_left):
        pl.semaphore_signal(barrier, inc=1, device_id={"tp": target}, device_id_type=MESH)

    def block_rows(slot):
        return pl.ds(pl.multiple_of(slot * block, block), block)

    own = pltpu.make_async_copy(weights, w_all.at[:, block_rows(sp), :], l_sem.at[0])
    own.start()
    own_tokens = pltpu.make_async_copy(tok, ext.at[pl.ds(HALO, rows)], l_sem.at[1])
    own_tokens.start()
    own.wait()
    pl.semaphore_wait(barrier, 6)

    def z_copy(d, step, p, distance):
        origin = around(z - distance, nz) if d == 0 else lax.rem(z + distance, nz)
        where = w_all.at[p, block_rows(origin * CORES + core), :]
        return pltpu.make_async_remote_copy(
            src_ref=where, dst_ref=where, send_sem=z_send.at[d, step, p], recv_sem=z_recv.at[d, step, p],
            device_id={"sp": z_next[d]}, device_id_type=MESH,
        )

    def p_copy(j, p, of_core):
        where = w_all.at[p, block_rows(lax.rem(z + j, nz) * CORES + of_core), :]
        return pltpu.make_async_remote_copy(
            src_ref=where, dst_ref=where, send_sem=p_send.at[j, p], recv_sem=p_recv.at[j, p],
            device_id={"sp": partner}, device_id_type=MESH,
        )

    steps = (nz // 2, nz - 1 - nz // 2)

    def landed(d, step, p):
        z_copy(d, step, p, step + 1).wait_recv()

    def share(d, step, p):
        p_copy(nz - 1 - step if d == 0 else step + 1, p, core).start()

    for p in range(PIECES):
        for d in range(2):
            z_copy(d, 0, p, 0).start()
    h_left = pltpu.make_async_remote_copy(
        src_ref=tok.at[pl.ds(0, HALO)], dst_ref=ext.at[pl.ds(HALO + rows, HALO)],
        send_sem=h_send.at[0], recv_sem=h_recv.at[0], device_id={"sp": seq_left}, device_id_type=MESH,
    )
    h_right = pltpu.make_async_remote_copy(
        src_ref=tok.at[pl.ds(rows - HALO, HALO)], dst_ref=ext.at[pl.ds(0, HALO)],
        send_sem=h_send.at[1], recv_sem=h_recv.at[1], device_id={"sp": seq_right}, device_id_type=MESH,
    )
    h_left.start()
    h_right.start()
    for p in range(PIECES):
        p_copy(0, p, core).start()

    own_tokens.wait()
    h_left.wait_recv()
    h_right.wait_recv()

    @pl.loop(0, ext.shape[0] // TILE)
    def _(t):
        where = pl.ds(pl.multiple_of(t * TILE, TILE), TILE)
        values = ext[where, :].astype(jnp.float32)
        scale = lax.rsqrt(jnp.mean(values * values, axis=-1, keepdims=True) + EPSILON)
        normed[where, :] = (values * scale * norm_gain[0:1, :]).astype(jnp.bfloat16)

    @pl.loop(1, steps[1])
    def _(step):
        for p in range(PIECES):
            for d in range(2):
                landed(d, step - 1, p)
                z_copy(d, step, p, step).start()
                share(d, step - 1, p)

    last = steps[1]
    for p in range(PIECES):
        landed(0, last - 1, p)
        z_copy(0, last, p, last).start()
        share(0, last - 1, p)
        landed(1, last - 1, p)
        share(1, last - 1, p)
    for p in range(PIECES):
        landed(0, last, p)
        share(0, last, p)

    @pl.loop(0, nz)
    def _(j):
        for p in range(PIECES):
            p_copy(j, p, 1 - core).wait_recv()

    half_window = jnp.left_shift(jnp.int32(1), me)

    for layer in range(LAYERS):
        extent = rows + 2 * HALO - 2 * REACH * layer
        count = extent - 2 * REACH
        half = half_rows(count)
        offset = HALO - REACH * layer
        first, second = pl.ds(0, half), pl.ds(half, count - half)

        if layer > 0:
            before = state[layer - 1]

            @pl.loop(0, extent // TILE)
            def _(t, before=before, layer=layer):
                where = pl.ds(pl.multiple_of(t * TILE, TILE), TILE)
                parts = [
                    before[k, c, where, :].astype(jnp.float32) for k in range(ntp) for c in range(CHUNKS)
                ]
                squares = parts[0] * parts[0]
                for part in parts[1:]:
                    squares = squares + part * part
                mean = jnp.sum(squares, axis=-1, keepdims=True) / model
                scale = lax.rsqrt(mean + EPSILON)
                for n, part in enumerate(parts):
                    columns = pl.ds(n * width, width)
                    gain = norm_gain[layer : layer + 1, columns]
                    normed[where, columns] = (part * scale * gain).astype(jnp.bfloat16)

        entered = jnp.dot(normed[0:extent, :], w_all[2 * layer], preferred_element_type=jnp.float32)
        at = sp * rows - offset + lax.broadcasted_iota(jnp.int32, (extent, 1), 0)
        inside = (at >= 0) & (at < total_length)
        pooled[0:extent, :] = jnp.where(inside, entered, 0.0).astype(jnp.bfloat16)

        here = lax.broadcasted_iota(jnp.int32, (count, extent), 0) + REACH
        there = lax.broadcasted_iota(jnp.int32, (count, extent), 1)
        apart = there - here
        band = jnp.where((apart >= -half_window) & (apart < half_window), 1.0, 0.0).astype(jnp.bfloat16)
        values = pooled[0:extent, :]
        summed = jnp.dot(band, values, preferred_element_type=jnp.float32)
        at = sp * rows - offset + REACH + lax.broadcasted_iota(jnp.int32, (count, 1), 0)
        lower = jnp.maximum(at - half_window, 0)
        upper = jnp.minimum(at + half_window, total_length)
        counted = jnp.maximum(upper - lower, 1).astype(jnp.float32)
        differ = summed / counted - values.astype(jnp.float32)[REACH : REACH + count]
        product = jnp.dot(differ.astype(jnp.bfloat16), mix[layer], preferred_element_type=jnp.float32)
        mixed[0:count, :] = (product * pool_gain[layer : layer + 1, :]).astype(jnp.bfloat16)

        def x_copy(c, m, layer=layer, first=first, second=second):
            t, a, s = term[layer], acc[layer], state[layer]
            source, target, to = (
                (t.at[c, tp_far, first], via_left[layer].at[c], tp_right),
                (t.at[c, tp_far, second], via_right[layer].at[c], tp_left),
                (t.at[c, tp_right, second], from_left[layer].at[c, second], tp_right),
                (t.at[c, tp_left, first], from_right[layer].at[c, first], tp_left),
                (a.at[c, first], from_left[layer].at[c, first], tp_right),
                (a.at[c, second], from_right[layer].at[c, second], tp_left),
                (s.at[me, c], s.at[me, c], tp_right),
                (s.at[me, c], s.at[me, c], tp_left),
                (s.at[tp_left, c, first], s.at[tp_left, c, first], tp_right),
                (s.at[tp_right, c, second], s.at[tp_right, c, second], tp_left),
            )[m]
            return pltpu.make_async_remote_copy(
                src_ref=source, dst_ref=target, send_sem=x_send.at[layer, c, m], recv_sem=x_recv.at[layer, c, m],
                device_id={"tp": to}, device_id_type=MESH,
            )

        def x_landed(c, m, layer=layer, first=first, second=second):
            s = state[layer]
            target = (
                via_left[layer].at[c],
                via_right[layer].at[c],
                from_left[layer].at[c, second],
                from_right[layer].at[c, first],
                from_left[layer].at[c, first],
                from_right[layer].at[c, second],
                s.at[tp_left, c],
                s.at[tp_right, c],
                s.at[tp_far, c, first],
                s.at[tp_far, c, second],
            )[m]
            pltpu.make_async_remote_copy(
                src_ref=target, dst_ref=target, send_sem=x_send.at[layer, c, m], recv_sem=x_recv.at[layer, c, m],
                device_id={"tp": tp_right}, device_id_type=MESH,
            ).wait_recv()

        def columns_of(k, c):
            return pl.ds(pl.multiple_of((k * CHUNKS + c) * width, width), width)

        def put(k, c, layer=layer):
            if layer == LAYERS - 1:
                pltpu.make_async_copy(state[layer].at[k, c], out.at[:, columns_of(k, c)], o_sem.at[k, c]).start()

        def compute_term(c, k, layer=layer, count=count):
            value = lax.dot_general(
                mixed[0:count, :], w_all[2 * layer + 1, columns_of(k, c), :], (((1,), (1,)), ((), ())),
                preferred_element_type=jnp.float32,
            )
            term[layer][c, k] = value.astype(jnp.bfloat16)

        for c in range(CHUNKS):
            compute_term(c, tp_far)
            x_copy(c, 0).start()
            x_copy(c, 1).start()
            compute_term(c, tp_right)
            x_copy(c, 2).start()
            compute_term(c, tp_left)
            x_copy(c, 3).start()
            compute_term(c, me)
        for c in range(CHUNKS):
            x_landed(c, 0)
            joined = term[layer][c, tp_right, first].astype(jnp.float32) + via_left[layer][c].astype(jnp.float32)
            acc[layer][c, first] = joined.astype(jnp.bfloat16)
            x_copy(c, 4).start()
            x_landed(c, 1)
            joined = term[layer][c, tp_left, second].astype(jnp.float32) + via_right[layer][c].astype(jnp.float32)
            acc[layer][c, second] = joined.astype(jnp.bfloat16)
            x_copy(c, 5).start()
        for c in range(CHUNKS):
            for m in (2, 3, 4, 5):
                x_landed(c, m)
            if layer == 0:
                kept = ext[:, columns_of(me, c)].astype(jnp.float32)
            else:
                kept = state[layer - 1][me, c].astype(jnp.float32)
            total = kept[REACH : REACH + count] + term[layer][c, me].astype(jnp.float32)
            total = total + from_left[layer][c].astype(jnp.float32) + from_right[layer][c].astype(jnp.float32)
            state[layer][me, c] = total.astype(jnp.bfloat16)
            x_copy(c, 6).start()
            x_copy(c, 7).start()
            put(me, c)
        for c in range(CHUNKS):
            x_landed(c, 6)
            x_copy(c, 8).start()
            put(tp_left, c)
            x_landed(c, 7)
            x_copy(c, 9).start()
            put(tp_right, c)
        for c in range(CHUNKS):
            x_landed(c, 8)
            x_landed(c, 9)
            put(tp_far, c)
        for c in range(CHUNKS):
            for m in range(10):
                x_copy(c, m).wait_send()

    h_left.wait_send()
    h_right.wait_send()

    @pl.loop(0, steps[1])
    def _(step):
        for p in range(PIECES):
            for d in range(2):
                z_copy(d, step, p, step).wait_send()

    @pl.loop(0, nz)
    def _(j):
        for p in range(PIECES):
            p_copy(j, p, core).wait_send()

    for p in range(PIECES):
        z_copy(0, last, p, last).wait_send()
    for k in range(ntp):
        for c in range(CHUNKS):
            pltpu.make_async_copy(state[-1].at[k, c], out.at[:, columns_of(k, c)], o_sem.at[k, c]).wait()


def per_device(nsp, ntp, tokens, norm_gain, entry_weight, mix_weight, pool_gain, back_weight):
    rows, model = tokens.shape
    pool = entry_weight.shape[2]
    turned = jnp.swapaxes(back_weight, 1, 2)
    weights = jnp.stack([entry_weight, turned], axis=1).reshape(PIECES, entry_weight.shape[1], pool)
    nz = nsp // CORES
    width = model // ntp // CHUNKS
    extent = rows + 2 * HALO
    counts = [rows + 2 * HALO - 2 * REACH * (layer + 1) for layer in range(LAYERS)]

    def per_layer(shape_of):
        return [pltpu.VMEM(shape_of(count), jnp.bfloat16) for count in counts]

    scratch = [
        pltpu.VMEM((extent, model), jnp.bfloat16),
        pltpu.VMEM((PIECES, model, pool), jnp.bfloat16),
        pltpu.VMEM((extent, model), jnp.bfloat16),
        pltpu.VMEM((extent, pool), jnp.bfloat16),
        pltpu.VMEM((extent, pool), jnp.bfloat16),
        *per_layer(lambda count: (CHUNKS, ntp, count, width)),
        *per_layer(lambda count: (CHUNKS, count, width)),
        *per_layer(lambda count: (CHUNKS, half_rows(count), width)),
        *per_layer(lambda count: (CHUNKS, count - half_rows(count), width)),
        *per_layer(lambda count: (CHUNKS, count, width)),
        *per_layer(lambda count: (CHUNKS, count, width)),
        *per_layer(lambda count: (ntp, CHUNKS, count, width)),
        pltpu.SemaphoreType.DMA((2, nz // 2, PIECES)),
        pltpu.SemaphoreType.DMA((2, nz // 2, PIECES)),
        pltpu.SemaphoreType.DMA((nz, PIECES)),
        pltpu.SemaphoreType.DMA((nz, PIECES)),
        pltpu.SemaphoreType.DMA((2,)),
        pltpu.SemaphoreType.DMA((2,)),
        pltpu.SemaphoreType.DMA((LAYERS, CHUNKS, 10)),
        pltpu.SemaphoreType.DMA((LAYERS, CHUNKS, 10)),
        pltpu.SemaphoreType.DMA((2,)),
        pltpu.SemaphoreType.DMA((ntp, CHUNKS)),
    ]
    anywhere = pl.BlockSpec(memory_space=pl.ANY)
    vmem = pl.BlockSpec(memory_space=pltpu.VMEM)
    return pl.pallas_call(
        functools.partial(kernel, nsp, ntp),
        out_shape=jax.ShapeDtypeStruct((rows, model), jnp.bfloat16),
        in_specs=[anywhere, anywhere, vmem, vmem, vmem],
        out_specs=anywhere,
        scratch_shapes=scratch,
        compiler_params=pltpu.CompilerParams(
            collective_id=0, has_side_effects=True, vmem_limit_bytes=56 * 2**20
        ),
        name="mixer",
    )(tokens, weights, norm_gain, mix_weight[:, 0], pool_gain)


def solution(mesh):
    body = functools.partial(per_device, mesh.shape["sp"], mesh.shape["tp"])
    return jax.shard_map(
        body,
        mesh=mesh,
        in_specs=(
            P(("grp", "sp"), None),
            P(),
            P(None, "sp", "tp"),
            P(None, "tp", None, None),
            P(None, "tp"),
            P(None, "tp", "sp"),
        ),
        out_specs=P(("grp", "sp"), None),
        check_vma=False,
    )
```

time: 393 us -> 183 us (0.47)
  Pallas kernels: 0 us -> 178 us
  waiting for transfers between devices: 166 us -> 0 us
  blocking collectives: 150 us -> 0 us
  matrix products: 24 us -> 0 us
  local copies, waits for them, and re-layouts: 19.9 us -> 3.39 us
  between operations: 13.7 us -> 0.01 us
  other arithmetic: 9.18 us -> 0.88 us
  starting transfers between devices: 6.9 us -> 0 us
    pallas_call x0 -> x1, Pallas kernels: none -> 178 us  [per_device(): pl.pallas_call(functools.partial(kernel, nsp, ntp), out_shape=jax.ShapeDt...]
    all_gather x1 -> x0, waiting for transfers between devices: 163 us -> none  [gather_turned(): out, at, done = (lax.all_gather(both, axis, axis=0, tiled=True), 0, [])]
    all_to_all x2 -> x0, blocking collectives: 150 us -> none  [from_everyone(): lax.all_to_all(jnp.broadcast_to(value[None], (length, *value.shape)), axi...]
    dot_general x4 -> x0, matrix products: 24 us -> none  [the longest x2 21.9 us: per_device(): update = jnp.dot(mixed, back_local, preferred_element_type=jnp.float32)]
    reshape x4 -> x0, local copies, waits for them, and re-layouts: 8.57 us -> none  [the longest x2 6.89 us: gather_turned(): section = out[:, at:at + t[0].size].reshape(-1, *t.shape[1:])]
    ppermute x4 -> x0, starting transfers between devices: 6.9 us -> none  [the longest x2 4.1 us: extended_2(): before = lax.ppermute(last, axis, up)]
    slice x5 -> x0, local copies, waits for them, and re-layouts: 6.81 us -> none  [the longest x1 5.22 us: gather_turned(): section = out[:, at:at + t[0].size].reshape(-1, *t.shape[1:])]
    reduce_sum x4 -> x0, other arithmetic: 4.87 us -> none  [the longest x2 2.54 us: over_copies(): return jnp.sum(everything.astype(jnp.float32), axis=0)]
  transfers between devices with their start and end apart: 5 -> 0, of which waited for: 2 -> 0; matrix products, arithmetic and copies ran while one was open for 3% -> 0% of each run, Pallas kernels for 0% -> 0%
where the time goes in v1:
time: 183 us
  Pallas kernels  178 us (97%)
  local copies, waits for them, and re-layouts  3.39 us (2%)
    pallas_call x1, Pallas kernels, per_device(): pl.pallas_call(functools.partial(kernel, nsp, ntp), out_shape=jax.ShapeDt...  178 us

profile of v1, /device:TPU:40, one launch (start us, length us, event | category | flops | bytes accessed | tf_op | source)
XLA Modules:
  0.0 182.6 jit_solution(13270124322988607105)
XLA Ops:
  0.0 0.9 pad_maximum_fusion
  0.9 0.7 copy.7
  1.6 178.3 %mixer.1 = bf16[384,2048]{1,0:T(8,128)(2,1)} custom-call(bf16[384,2048]{1,0:T(8,128)(2,1)} %tok.1, bf16[4,32,512]{2,1,0:T(8,128)(2,1)} %bitcast.7, f32[2,2048]{1,0:T(2,128)} %norm_gain.1, bf16[2,512,512]{2,1,0:T(8,128)(2,1)} %bitcast.6, f32[2,512]{1,0:T(2,128)} %pool_gain.1), custom_call_target="tpu_custom_call" | custom-call | tf_op jit(solution)/shard_map/mixer/pallas_call | solution.py:350
  179.8 2.7 %copy.9 = bf16[384,2048]{1,0:T(8,128)(2,1)} copy(bf16[384,2048]{1,0:T(8,128)(2,1)} %mixer.1) | data formatting | bytes 3145728
